TPU v7x, 32 devices: a whole 2x2x4 slice. The times are simulated.
32 devices in a mesh: sp: 16 (over z, y, core), tp: 2 (over x).
Axes of the slice: x: 2, y: 2, z: 4, core: 2. Of those that a mesh axis runs over, the one named last changes fastest.
Arguments:
- queries: bfloat16 [16384, 1024], P('sp', 'tp'), may hold values from -8 to 8
- keys: bfloat16 [16384, 256], P('sp', 'tp'), may hold values from -8 to 8
- values: bfloat16 [16384, 256], P('sp', 'tp'), may hold values from -18 to 18
- doc_ids: int32 [16384], P('sp'), may hold values from 0 to 3, never falling along the last dimension, each value on 1 to 8192 neighbouring positions
- sinks: float32 [16], P('tp'), may hold values from 0 to 4
- residual: bfloat16 [16384, 2048], P(('sp', 'tp')), may hold values from -12 to 12
- out_weight: bfloat16 [1024, 2048], P('tp'), may hold values from -0.1875 to 0.1875
- norm_gain: float32 [2048], replicated, may hold values from 0.1 to 1.9
- w_gate: bfloat16 [2048, 5632], P('sp', 'tp'), may hold values from -0.125 to 0.125
- w_value: bfloat16 [2048, 5632], P('sp', 'tp'), may hold values from -0.125 to 0.125
- conv_gate: float32 [3, 5632], P(None, 'tp'), may hold values from -3.5 to 3.5
- conv_value: float32 [3, 5632], P(None, 'tp'), may hold values from -3.5 to 3.5
- w_down: bfloat16 [5632, 2048], P('tp', 'sp'), may hold values from -0.078125 to 0.078125
Outputs:
- layer_out: bfloat16 [16384, 2048], P(('sp', 'tp'))
All inputs are finite; a program needn't handle non-finite values.
Results may differ from a plain program's by a relative error of at most 0.012.
Values may be sent and summed in bfloat16 or wider, within the bound.
A program may use at most 128 MiB of HBM per device.

v0:
```python
import jax
import jax.numpy as jnp
from jax import lax
from jax.sharding import PartitionSpec as P

HEAD_DIM = 64
WINDOW = 128


def shifted(shard, axis, by):
    size = lax.axis_size(axis)
    pairs = [(i, i + by) for i in range(size) if 0 <= i + by < size]
    return lax.ppermute(shard, axis, pairs)


def attend(query_rows, key_ext, value_ext, doc_rows, doc_ext, sinks):
    row_count = query_rows.shape[0]
    block_count = row_count // WINDOW
    kv_heads = key_ext.shape[1] // HEAD_DIM
    group_size = query_rows.shape[1] // (kv_heads * HEAD_DIM)

    def band(t):
        lower = t[:row_count].reshape((block_count, WINDOW) + t.shape[1:])
        upper = t[WINDOW:].reshape((block_count, WINDOW) + t.shape[1:])
        return jnp.concatenate([lower, upper], axis=1)

    query_band = query_rows.reshape(block_count, WINDOW, kv_heads, group_size, HEAD_DIM)
    key_band = band(key_ext).reshape(block_count, 2 * WINDOW, kv_heads, HEAD_DIM)
    value_band = band(value_ext).reshape(block_count, 2 * WINDOW, kv_heads, HEAD_DIM)
    doc_band = band(doc_ext)
    distance = jnp.arange(WINDOW)[:, None] + WINDOW - jnp.arange(2 * WINDOW)[None, :]
    in_window = (distance >= 0) & (distance < WINDOW)
    same_doc = doc_rows.reshape(block_count, WINDOW)[:, :, None] == doc_band[:, None, :]
    keep_mask = in_window[None] & same_doc
    scores = jnp.einsum(
        "nqhgd,nkhd->nhgqk", query_band, key_band, preferred_element_type=jnp.float32
    ) * HEAD_DIM ** (-0.5)
    scores = jnp.where(keep_mask[:, None, None], scores, -jnp.inf)
    sink_logit = sinks.reshape(kv_heads, group_size)[None, :, :, None, None]
    peak = jnp.maximum(jnp.max(scores, axis=-1, keepdims=True), sink_logit)
    expd = jnp.exp(scores - peak)
    probs = (expd / (jnp.sum(expd, axis=-1, keepdims=True) + jnp.exp(sink_logit - peak))).astype(
        jnp.bfloat16
    )
    mixed = jnp.einsum("nhgqk,nkhd->nqhgd", probs, value_band, preferred_element_type=jnp.float32)
    return mixed.astype(jnp.bfloat16).reshape(row_count, -1)


def convolve(ext_rows, doc_ext, taps):
    center = doc_ext[2:]
    same_one = (doc_ext[1:-1] == center)[:, None]
    same_two = (doc_ext[:-2] == center)[:, None]
    ext32 = ext_rows.astype(jnp.float32)
    result = taps[2] * ext32[2:]
    result = result + jnp.where(same_one, taps[1] * ext32[1:-1], 0.0)
    return result + jnp.where(same_two, taps[0] * ext32[:-2], 0.0)


def per_device(
    queries,
    keys,
    values,
    doc_ids,
    sinks,
    residual,
    out_weight,
    norm_gain,
    w_gate,
    w_value,
    conv_gate,
    conv_value,
    w_down,
):
    docs_plus = doc_ids + 1
    prev_keys, prev_values, prev_docs = shifted(
        (keys[-WINDOW:], values[-WINDOW:], docs_plus[-WINDOW:]), "sp", 1
    )
    key_ext = jnp.concatenate([prev_keys, keys], axis=0)
    value_ext = jnp.concatenate([prev_values, values], axis=0)
    doc_ext = jnp.concatenate([prev_docs, docs_plus], axis=0)
    head_out = attend(queries, key_ext, value_ext, docs_plus, doc_ext, sinks)
    head_rows = lax.all_to_all(head_out, "tp", split_axis=0, concat_axis=1, tiled=True)
    proj = jnp.dot(
        head_rows,
        lax.all_gather(out_weight, "tp", axis=0, tiled=True),
        preferred_element_type=jnp.float32,
    )
    mid32 = (residual.astype(jnp.float32) + proj).astype(jnp.bfloat16).astype(jnp.float32)
    normed = (
        mid32 * lax.rsqrt(jnp.mean(mid32 * mid32, axis=-1, keepdims=True) + 1e-06) * norm_gain
    ).astype(jnp.bfloat16)
    whole = lax.all_gather(normed, "tp", axis=0, tiled=True)

    def add_rows(piece):
        return jnp.dot(whole, piece, preferred_element_type=jnp.float32)

    gate_sum = add_rows(lax.all_gather(w_gate, "sp", axis=0, tiled=True))
    value_sum = add_rows(lax.all_gather(w_value, "sp", axis=0, tiled=True))
    gate_pre = gate_sum.astype(jnp.bfloat16)
    value_pre = value_sum.astype(jnp.bfloat16)
    prev_gate, prev_value = shifted((gate_pre[-2:], value_pre[-2:]), "sp", 1)
    conv_docs = jnp.concatenate([prev_docs[-2:], docs_plus], axis=0)
    gate_conv = convolve(jnp.concatenate([prev_gate, gate_pre], axis=0), conv_docs, conv_gate)
    value_conv = convolve(jnp.concatenate([prev_value, value_pre], axis=0), conv_docs, conv_value)
    hidden = (jax.nn.silu(gate_conv) * value_conv).astype(jnp.bfloat16)
    terms = jnp.dot(
        hidden, lax.all_gather(w_down, "sp", axis=1, tiled=True), preferred_element_type=jnp.float32
    )
    sums = lax.psum_scatter(
        terms.astype(jnp.bfloat16), "tp", scatter_dimension=0, tiled=True
    ).astype(jnp.float32)
    return (mid32 + sums).astype(jnp.bfloat16)


def solution(mesh):
    return jax.shard_map(
        per_device,
        mesh=mesh,
        in_specs=(
            P("sp", "tp"),
            P("sp", "tp"),
            P("sp", "tp"),
            P("sp"),
            P("tp"),
            P(("sp", "tp"), None),
            P("tp", None),
            P(),
            P("sp", "tp"),
            P("sp", "tp"),
            P(None, "tp"),
            P(None, "tp"),
            P("tp", "sp"),
        ),
        out_specs=P(("sp", "tp"), None),
        check_vma=False,
    )
```

profile of v0, /device:TPU:0, one launch (start us, length us, event | category | flops | bytes accessed | tf_op | source)
XLA Modules:
  0.0 544.3 jit_solution(59607860426561)
XLA Ops:
  6.5 0.7 broadcast_add_fusion
  7.3 0.5 slice.83
  7.8 2.4 collective-permute-start.1
  10.2 1.4 slice.86
  11.6 4.5 collective-permute-start.2
  16.1 0.8 slice.81
  16.9 1.9 collective-permute-start
  18.9 1.2 reshape.97
  20.1 1.2 reshape.95
  21.3 3.5 reshape.98
  24.9 1.0 copy.36
  25.8 0.7 max.18
  26.6 1.0 copy.32
  27.6 0.3 compare_and_fusion
  28.0 0.2 reshape.96
  28.2 0.4 copy.35
  28.6 1.0 pad_maximum_fusion.1
  29.6 0.2 reshape.94
  29.9 0.4 copy.31
  30.3 2.6 fusion.11
  33.0 2.3 fusion.10
  35.3 0.1 exponential_add_fusion
  35.4 2.4 fusion.25
  37.8 0.7 copy.40
  38.5 0.4 all_to_all.14
  39.0 0.2 copy.41
  39.1 28.8 %all_to_all.19 = bf16[2,512,512]{1,2,0:T(8,128)(2,1)S(1)} all-to-all(bf16[2,512,512]{1,2,0:T(8,128)(2,1)S(1)} %copy.41), channel_id=1, replica_groups=mesh['sp'=16,'tp'=2] {'tp'}, dimensions={0} | all-to-all | bytes 2097152 | tf_op jit(solution)/shard_map/all_to_all | solution.py:82
  67.9 20.5 %all-gather.6.cloned.1.call-done = bf16[1024,2048]{1,0:T(8,128)(2,1)} async-done(((bf16[512,2048]{1,0:T(8,128)(2,1)}), bf16[1024,2048]{1,0:T(8,128)(2,1)}) %all-gather.6.cloned.1.call-update) | async-done | bytes 4194320 | tf_op jit(solution)/shard_map/all_gather | solution.py:85
  88.4 5.6 %fusion.14 = (f32[512]{0:T(512)S(1)}, bf16[512,2048]{1,0:T(8,128)(2,1)S(1)}) fusion(bf16[512,1024]{0,1:T(8,128)(2,1)S(1)} %bitcast.45, bf16[1024,2048]{1,0:T(8,128)(2,1)} %all-gather.6.cloned.1.call-done, bf16[512,2048]{1,0:T(8,128)(2,1)} %param.18), kind=kOutput, calls=%fused_computation.29 | convolution fusion | flops 2153774592 | bytes 9439232 | tf_op jit(solution)/shard_map/dot_general | solution.py:83
  94.1 1.9 fusion.16
  96.0 0.7 all-gather.10.cloned.1.call-update
  96.8 0.5 all-gather.12.cloned.1.call-update
  97.3 0.5 all-gather.14.cloned.1.call-update
  98.0 0.2 slice_reduce_fusion.2
  98.3 54.6 %all-gather.8.cloned.1.call-done = bf16[1024,2048]{1,0:T(8,128)(2,1)} async-done(((bf16[512,2048]{1,0:T(8,128)(2,1)}), bf16[1024,2048]{1,0:T(8,128)(2,1)}) %all-gather.8.cloned.1.call-update) | async-done | bytes 4194320 | tf_op jit(solution)/shard_map/all_gather | solution.py:92
  152.9 96.3 %all-gather.10.cloned.1.call-done = bf16[2048,2816]{1,0:T(8,128)(2,1)} async-done(((bf16[128,2816]{1,0:T(8,128)(2,1)}), bf16[2048,2816]{1,0:T(8,128)(2,1)}) %all-gather.10.cloned.1.call-update) | async-done | bytes 11534352 | tf_op jit(solution)/shard_map/all_gather | solution.py:97
  249.2 17.0 %convolution_convert_fusion.1 = bf16[1024,2816]{1,0:T(8,128)(2,1)S(1)} fusion(bf16[1024,2048]{1,0:T(8,128)(2,1)} %all-gather.8.cloned.1.call-done, bf16[2048,2816]{1,0:T(8,128)(2,1)} %all-gather.10.cloned.1.call-done), kind=kOutput, calls=%fused_computation.28 | convolution fusion | flops 11814043648 | bytes 21495808 | tf_op jit(solution)/shard_map/dot_general | solution.py:95
  266.2 2.5 copy-done
  268.7 2.2 collective-permute-start.3
  270.9 72.8 %all-gather.12.cloned.1.call-done = bf16[2048,2816]{1,0:T(8,128)(2,1)} async-done(((bf16[128,2816]{1,0:T(8,128)(2,1)}), bf16[2048,2816]{1,0:T(8,128)(2,1)}) %all-gather.12.cloned.1.call-update) | async-done | bytes 11534352 | tf_op jit(solution)/shard_map/all_gather | solution.py:98
  343.7 17.1 %convolution_convert_fusion = bf16[1024,2816]{1,0:T(8,128)(2,1)S(1)} fusion(bf16[1024,2048]{1,0:T(8,128)(2,1)} %all-gather.8.cloned.1.call-done, bf16[2048,2816]{1,0:T(8,128)(2,1)} %all-gather.12.cloned.1.call-done), kind=kOutput, calls=%fused_computation.27 | convolution fusion | flops 11814043648 | bytes 21495808 | tf_op jit(solution)/shard_map/dot_general | solution.py:95
  360.9 2.4 collective-permute-start.4
  363.3 5.5 %maximum_convert_fusion = f32[1026,2816]{1,0:T(8,128)} fusion(bf16[1024,2816]{1,0:T(8,128)(2,1)S(1)} %copy-done.1, bf16[2,2816]{1,0:T(2,128)(2,1)S(1)} %collective-permute-done.3), kind=kLoop, calls=%fused_computation.24 | loop fusion | flops 11556864 | bytes 17335296 | tf_op jit(solution)/shard_map/convert_element_type | solution.py:53
  368.7 5.5 %maximum_convert_fusion.1 = f32[1026,2816]{1,0:T(8,128)} fusion(bf16[1024,2816]{1,0:T(8,128)(2,1)S(1)} %convolution_convert_fusion, bf16[2,2816]{1,0:T(2,128)(2,1)S(1)} %collective-permute-done.4), kind=kLoop, calls=%fused_computation.25 | loop fusion | flops 11556864 | bytes 17335296 | tf_op jit(solution)/shard_map/convert_element_type | solution.py:53
  374.2 66.7 %all-gather.14.cloned.1.call-done = bf16[2816,2048]{1,0:T(8,128)(2,1)} async-done(((bf16[2816,128]{1,0:T(8,128)(2,1)}), bf16[2816,2048]{1,0:T(8,128)(2,1)}) %all-gather.14.cloned.1.call-update) | async-done | bytes 11534352 | tf_op jit(solution)/shard_map/all_gather | solution.py:107
  440.9 40.0 %fusion.19 = bf16[1024,2048]{1,0:T(8,128)(2,1)} fusion(bf16[2816,2048]{1,0:T(8,128)(2,1)} %all-gather.14.cloned.1.call-done, f32[1026,2816]{1,0:T(8,128)} %maximum_convert_fusion.1, f32[1026,2816]{1,0:T(8,128)} %maximum_convert_fusion, f32[2816]{0:T(1024)S(1)} %get-tuple-element.9, f32[2816]{0:T(1024)S(1)} %get-tuple-element.10, ...), kind=kOutput, calls=%fused_computation.35 | convolution fusion | flops 11870928896 | bytes 85004288 | tf_op jit(solution)/shard_map/dot_general | solution.py:106
  480.9 52.7 %reduce-scatter.2.cloned.1.call-done = bf16[512,2048]{1,0:T(8,128)(2,1)} async-done(((bf16[1024,2048]{1,0:T(8,128)(2,1)}), bf16[512,2048]{1,0:T(8,128)(2,1)}) %reduce-scatter.2.cloned.1.call-update) | async-done | bytes 2097168 | tf_op jit(solution)/shard_map/reduce_scatter | solution.py:109
  533.6 3.8 fusion.17
  (38 shorter events, 0.6 us)
Async XLA Ops:
  6.5 21.4 %copy-start.2 = (bf16[1024,128]{1,0:T(8,128)(2,1)S(1)}, bf16[1024,128]{1,0:T(8,128)(2,1)}, u32[]{:S(2)}) copy-start(bf16[1024,128]{1,0:T(8,128)(2,1)} %param.14) | copy-start | bytes 786436
  6.5 81.9 %all-gather.6.cloned.1.call-start = ((), (), s32[]{:S(2)}) async-start(), calls=%async_computation.2 | async-start | bytes 6291456 | tf_op jit(solution)/shard_map/all_gather | solution.py:85
  7.8 19.7 %collective-permute-start.1 = (s32[128]{0:T(128)}, s32[128]{0:T(128)S(1)}, u32[]{:S(2)}, u32[]{:S(2)}) collective-permute-start(s32[128]{0:T(128)} %slice.83), channel_id=1, source_target_pairs={{0,2},{2,4},{4,6},{6,8},{8,10},{10,12},{12,14},{14,16},{16,18},{18... | collective-permute-start | bytes 1544 | tf_op jit(solution)/shard_map/ppermute | solution.py:13
  11.6 16.4 %collective-permute-start.2 = (bf16[128,128]{1,0:T(8,128)(2,1)}, bf16[128,128]{1,0:T(8,128)(2,1)S(1)}, u32[]{:S(2)}, u32[]{:S(2)}) collective-permute-start(bf16[128,128]{1,0:T(8,128)(2,1)} %slice.86), channel_id=1, source_target_pairs={{0,2},{2,4},{4,6},{6,8},{8,10},{10,12},{12,14},{14,16},{16,18},{18... | collective-permute-start | bytes 98312 | tf_op jit(solution)/shard_map/ppermute | solution.py:13
  16.9 11.7 %collective-permute-start = (bf16[128,128]{1,0:T(8,128)(2,1)S(1)}, bf16[128,128]{1,0:T(8,128)(2,1)S(1)}, u32[]{:S(2)}, u32[]{:S(2)}) collective-permute-start(bf16[128,128]{1,0:T(8,128)(2,1)S(1)} %slice.81), channel_id=1, source_target_pairs={{0,2},{2,4},{4,6},{6,8},{8,10},{10,12},{12,14},{14,16},{16,18},{18... | collective-permute-start | bytes 98312 | tf_op jit(solution)/shard_map/ppermute | solution.py:13
  18.8 134.1 %all-gather.8.cloned.1.call-start = ((), (), s32[]{:S(2)}) async-start(), calls=%async_computation.3 | async-start | bytes 6291456 | tf_op jit(solution)/shard_map/all_gather | solution.py:92
  30.3 5.1 copy-start.3
  39.0 55.1 %copy-start.6 = (f32[2048]{0:T(1024)S(1)}, f32[2048]{0:T(1024)}, u32[]{:S(2)}) copy-start(f32[2048]{0:T(1024)} %param.20) | copy-start | bytes 24580
  88.4 9.5 %copy-start.4 = (f32[3,2816]{1,0:T(4,128)S(1)}, f32[3,2816]{1,0:T(4,128)}, u32[]{:S(2)}) copy-start(f32[3,2816]{1,0:T(4,128)} %param.24) | copy-start | bytes 101380
  88.4 9.5 %copy-start.5 = (f32[3,2816]{1,0:T(4,128)S(1)}, f32[3,2816]{1,0:T(4,128)}, u32[]{:S(2)}) copy-start(f32[3,2816]{1,0:T(4,128)} %param.23) | copy-start | bytes 101380
  96.0 153.2 %all-gather.10.cloned.1.call-start = ((), (), s32[]{:S(2)}) async-start(), calls=%async_computation.4 | async-start | bytes 12255232 | tf_op jit(solution)/shard_map/all_gather | solution.py:97
  96.7 247.0 %all-gather.12.cloned.1.call-start = ((), (), s32[]{:S(2)}) async-start(), calls=%async_computation.5 | async-start | bytes 12255232 | tf_op jit(solution)/shard_map/all_gather | solution.py:98
  97.3 343.6 %all-gather.14.cloned.1.call-start = ((), (), s32[]{:S(2)}) async-start(), calls=%async_computation.6 | async-start | bytes 12255232 | tf_op jit(solution)/shard_map/all_gather | solution.py:107
  97.9 435.7 %reduce-scatter.2.cloned.1.call-start = ((), (), s32[]{:S(2)}) async-start(), calls=%async_computation.7 | async-start | bytes 6291456 | tf_op jit(solution)/shard_map/reduce_scatter | solution.py:109
  266.2 2.5 copy-start
  268.7 94.5 %collective-permute-start.3 = (bf16[2,2816]{1,0:T(2,128)(2,1)S(1)}, bf16[2,2816]{1,0:T(2,128)(2,1)S(1)}, u32[]{:S(2)}, u32[]{:S(2)}) collective-permute-start(bf16[2,2816]{1,0:T(2,128)(2,1)S(1)} %slice.105), channel_id=1, source_target_pairs={{0,2},{2,4},{4,6},{6,8},{8,10},{10,12},{12,14},{14,16},{16,18},{18... | collective-permute-start | bytes 33800 | tf_op jit(solution)/shard_map/ppermute | solution.py:13
  343.7 19.6 %copy-start.1 = (bf16[1024,2816]{1,0:T(8,128)(2,1)S(1)}, bf16[1024,2816]{1,0:T(8,128)(2,1)}, u32[]{:S(2)}) copy-start(bf16[1024,2816]{1,0:T(8,128)(2,1)} %copy-done) | copy-start | bytes 17301508
  360.9 7.9 %collective-permute-start.4 = (bf16[2,2816]{1,0:T(2,128)(2,1)S(1)}, bf16[2,2816]{1,0:T(2,128)(2,1)S(1)}, u32[]{:S(2)}, u32[]{:S(2)}) collective-permute-start(bf16[2,2816]{1,0:T(2,128)(2,1)S(1)} %slice.111), channel_id=1, source_target_pairs={{0,2},{2,4},{4,6},{6,8},{8,10},{10,12},{12,14},{14,16},{16,18},{18... | collective-permute-start | bytes 33800 | tf_op jit(solution)/shard_map/ppermute | solution.py:13
Sparse Core Ops, SparseCore 0:
  18.9 69.4 all-gather.5
  96.1 56.7 all-gather.7
  155.1 93.9 all-gather.9
  251.3 92.3 all-gather.11
  345.7 95.1 all-gather.13
  481.0 52.5 reduce-scatter.1
where the time goes:
time: 545 us; the launch traced here: 544 us
  waiting for transfers between devices  365 us (67%)
  matrix products  84.8 us (16%)
  blocking collectives  28.8 us (5%)
  other arithmetic  21.3 us (4%)
  local copies, waits for them, and re-layouts  16.6 us (3%)
  between operations  13.8 us (3%)
  starting transfers between devices  13.5 us (2%)
    all_gather x1, waiting for transfers between devices, per_device(): gate_sum = add_rows(lax.all_gather(w_gate, 'sp', axis=0, tiled=True))  96.3 us
    all_gather x1, waiting for transfers between devices, per_device(): value_sum = add_rows(lax.all_gather(w_value, 'sp', axis=0, tiled=True))  72.8 us
    all_gather x1, waiting for transfers between devices, per_device(): lax.all_gather(w_down, 'sp', axis=1, tiled=True)  66.7 us
    all_gather x1, waiting for transfers between devices, per_device(): whole = lax.all_gather(normed, 'tp', axis=0, tiled=True)  54.6 us
    reduce_scatter x1, waiting for transfers between devices, per_device(): lax.psum_scatter(terms.astype(jnp.bfloat16), 'tp', scatter_dimension=0, t...  52.7 us
    dot_general x1, matrix products, per_device(): jnp.dot(hidden, lax.all_gather(w_down, 'sp', axis=1, tiled=True), preferr...  40 us
    dot_general x2, matrix products, add_rows(): return jnp.dot(whole, piece, preferred_element_type=jnp.float32)  34.2 us
    all_to_all x1, blocking collectives, per_device(): lax.all_to_all(head_out, 'tp', split_axis=0, concat_axis=1, tiled=True)  28.8 us
  transfers between devices with their start and end apart: 11, of which 6 were waited for; matrix products, arithmetic and copies ran while one was open for 12% of the time, Pallas kernels for 0%

commit v1 on v0

--- a/solution.py
+++ b/solution.py
@@ -104,7 +104,9 @@
     value_conv = convolve(jnp.concatenate([prev_value, value_pre], axis=0), conv_docs, conv_value)
     hidden = (jax.nn.silu(gate_conv) * value_conv).astype(jnp.bfloat16)
     terms = jnp.dot(
-        hidden, lax.all_gather(w_down, "sp", axis=1, tiled=True), preferred_element_type=jnp.float32
+        hidden,
+        jnp.concatenate(lax.all_gather(w_down, "sp"), axis=1),
+        preferred_element_type=jnp.float32,
     )
     sums = lax.psum_scatter(
         terms.astype(jnp.bfloat16), "tp", scatter_dimension=0, tiled=True

time: 545 us -> 581 us (1.066)
  local copies, waits for them, and re-layouts: 16.6 us -> 32.6 us
  waiting for transfers between devices: 365 us -> 376 us
  matrix products: 84.8 us -> 91.7 us
    all_gather x1, waiting for transfers between devices: 72.8 us -> 96.3 us  [per_device(): value_sum = add_rows(lax.all_gather(w_value, 'sp', axis=0, tiled=True))]
    all_gather x1, waiting for transfers between devices: 96.3 us -> 72.8 us  [per_device(): gate_sum = add_rows(lax.all_gather(w_gate, 'sp', axis=0, tiled=True))]
    reshape x0 -> x1, local copies, waits for them, and re-layouts: none -> 15 us  [per_device(): jnp.concatenate(lax.all_gather(w_down, 'sp'), axis=1)]
    all_gather x1, waiting for transfers between devices: 66.7 us -> 75.9 us  [per_device(): lax.all_gather(w_down, 'sp')]
  transfers between devices with their start and end apart: 11 -> 11, of which waited for: 6 -> 6; matrix products, arithmetic and copies ran while one was open for 12% -> 14% of each run, Pallas kernels for 0% -> 0%
where the time goes in v1:
time: 581 us; the launch traced here: 580 us
  waiting for transfers between devices  376 us (65%)
  matrix products  91.7 us (16%)
  local copies, waits for them, and re-layouts  32.6 us (6%)
  blocking collectives  28.8 us (5%)
  other arithmetic  23.8 us (4%)
  between operations  13.8 us (2%)
  starting transfers between devices  13.7 us (2%)
    all_gather x1, waiting for transfers between devices, per_device(): value_sum = add_rows(lax.all_gather(w_value, 'sp', axis=0, tiled=True))  96.3 us
    all_gather x1, waiting for transfers between devices, per_device(): lax.all_gather(w_down, 'sp')  75.9 us
    all_gather x1, waiting for transfers between devices, per_device(): gate_sum = add_rows(lax.all_gather(w_gate, 'sp', axis=0, tiled=True))  72.8 us
    all_gather x1, waiting for transfers between devices, per_device(): whole = lax.all_gather(normed, 'tp', axis=0, tiled=True)  54.6 us
    reduce_scatter x1, waiting for transfers between devices, per_device(): lax.psum_scatter(terms.astype(jnp.bfloat16), 'tp', scatter_dimension=0, t...  53.8 us
    dot_general x1, matrix products, per_device(): jnp.dot(hidden, jnp.concatenate(lax.all_gather(w_down, 'sp'), axis=1), pr...  45.5 us
    dot_general x2, matrix products, add_rows(): return jnp.dot(whole, piece, preferred_element_type=jnp.float32)  35.5 us
    all_to_all x1, blocking collectives, per_device(): lax.all_to_all(head_out, 'tp', split_axis=0, concat_axis=1, tiled=True)  28.8 us
  transfers between devices with their start and end apart: 11, of which 6 were waited for; matrix products, arithmetic and copies ran while one was open for 14% of the time, Pallas kernels for 0%

profile of v1, /device:TPU:0, one launch (start us, length us, event | category | flops | bytes accessed | tf_op | source)
XLA Modules:
  0.0 580.0 jit_solution(3146788316016367210)
XLA Ops:
  6.5 0.7 broadcast_add_fusion
  7.3 0.6 slice.83
  7.8 2.4 collective-permute-start.1
  10.2 1.4 slice.86
  11.6 4.5 collective-permute-start.2
  16.1 0.8 slice.81
  16.9 1.9 collective-permute-start
  18.9 1.2 reshape.106
  20.1 1.2 reshape.104
  21.4 3.5 reshape.107
  24.9 1.0 copy.50
  25.9 0.7 max.18
  26.6 1.0 copy.46
  27.6 0.3 compare_and_fusion
  28.0 0.2 reshape.105
  28.3 0.4 copy.49
  28.6 1.0 pad_maximum_fusion.1
  29.7 0.2 reshape.103
  29.9 0.4 copy.45
  30.3 2.6 fusion.11
  33.0 2.3 fusion.10
  35.4 2.4 fusion.25
  37.9 0.7 copy.54
  38.5 0.4 all_to_all.14
  39.2 28.8 %all_to_all.19 = bf16[2,512,512]{1,2,0:T(8,128)(2,1)S(1)} all-to-all(bf16[2,512,512]{1,2,0:T(8,128)(2,1)S(1)} %copy.55), channel_id=1, replica_groups=mesh['sp'=16,'tp'=2] {'tp'}, dimensions={0} | all-to-all | bytes 2097152 | tf_op jit(solution)/shard_map/all_to_all | solution.py:82
  68.0 20.5 %all-gather.7.cloned.1.call-done = bf16[1024,2048]{1,0:T(8,128)(2,1)} async-done(((bf16[512,2048]{1,0:T(8,128)(2,1)}), bf16[1024,2048]{1,0:T(8,128)(2,1)}) %all-gather.7.cloned.1.call-update) | async-done | bytes 4194320 | tf_op jit(solution)/shard_map/all_gather | solution.py:85
  88.5 5.6 fusion.14
  94.1 1.9 fusion.16
  96.1 0.7 all-gather.13.cloned.1.call-update
  96.8 0.5 all-gather.11.cloned.1.call-update
  97.4 0.5 all-gather.15.cloned.1.call-update
  98.0 0.2 slice_reduce_fusion.2
  98.3 54.6 %all-gather.9.cloned.1.call-done = bf16[1024,2048]{1,0:T(8,128)(2,1)} async-done(((bf16[512,2048]{1,0:T(8,128)(2,1)}), bf16[1024,2048]{1,0:T(8,128)(2,1)}) %all-gather.9.cloned.1.call-update) | async-done | bytes 4194320 | tf_op jit(solution)/shard_map/all_gather | solution.py:92
  152.9 96.3 %all-gather.13.cloned.1.call-done = bf16[2048,2816]{1,0:T(8,128)(2,1)} async-done(((bf16[128,2816]{1,0:T(8,128)(2,1)}), bf16[2048,2816]{1,0:T(8,128)(2,1)}) %all-gather.13.cloned.1.call-update) | async-done | bytes 11534352 | tf_op jit(solution)/shard_map/all_gather | solution.py:98
  249.2 17.0 %convolution_convert_fusion = bf16[1024,2816]{1,0:T(8,128)(2,1)S(1)} fusion(bf16[1024,2048]{1,0:T(8,128)(2,1)} %all-gather.9.cloned.1.call-done, bf16[2048,2816]{1,0:T(8,128)(2,1)} %all-gather.13.cloned.1.call-done), kind=kOutput, calls=%fused_computation.27 | convolution fusion | flops 11814043648 | bytes 21495808 | tf_op jit(solution)/shard_map/dot_general | solution.py:95
  266.2 2.5 copy-done
  268.7 2.2 collective-permute-start.4
  270.9 72.8 %all-gather.11.cloned.1.call-done = bf16[2048,2816]{1,0:T(8,128)(2,1)} async-done(((bf16[128,2816]{1,0:T(8,128)(2,1)}), bf16[2048,2816]{1,0:T(8,128)(2,1)}) %all-gather.11.cloned.1.call-update) | async-done | bytes 11534352 | tf_op jit(solution)/shard_map/all_gather | solution.py:97
  343.7 18.5 %convolution_convert_fusion.1 = bf16[1024,2816]{1,0:T(8,128)(2,1)} fusion(bf16[1024,2048]{1,0:T(8,128)(2,1)} %all-gather.9.cloned.1.call-done, bf16[2048,2816]{1,0:T(8,128)(2,1)} %all-gather.11.cloned.1.call-done), kind=kOutput, calls=%fused_computation.28 | convolution fusion | flops 11814043648 | bytes 21495808 | tf_op jit(solution)/shard_map/dot_general | solution.py:95
  362.2 75.9 %all-gather.15.cloned.1.call-done = bf16[45056,128]{1,0:T(8,128)(2,1)} async-done(((bf16[2816,128]{1,0:T(8,128)(2,1)}), bf16[45056,128]{1,0:T(8,128)(2,1)}) %all-gather.15.cloned.1.call-update) | async-done | bytes 11534352 | tf_op jit(solution)/shard_map/all_gather | solution.py:108
  438.1 15.0 %copy.56 = bf16[2816,16,128]{0,2,1:T(8,128)(2,1)} copy(bf16[2816,16,128]{2,0,1:T(8,128)(2,1)} %bitcast.49) | data formatting | bytes 23068672 | tf_op jit(solution)/shard_map/reshape | solution.py:108
  453.1 1.0 slice.105
  454.1 2.5 collective-permute-start.3
  456.6 8.1 %maximum_convert_fusion.1 = f32[1026,2816]{1,0:T(8,128)} fusion(bf16[1024,2816]{1,0:T(8,128)(2,1)} %copy-done, bf16[2,2816]{1,0:T(2,128)(2,1)S(1)} %collective-permute-done.4), kind=kLoop, calls=%fused_computation.25 | loop fusion | flops 11556864 | bytes 17335296 | tf_op jit(solution)/shard_map/convert_element_type | solution.py:53
  464.8 5.4 maximum_convert_fusion
  470.1 45.5 %fusion.19 = bf16[1024,2048]{1,0:T(8,128)(2,1)} fusion(bf16[2816,2048]{0,1:T(8,128)(2,1)} %bitcast.50, f32[1026,2816]{1,0:T(8,128)} %maximum_convert_fusion.1, f32[1026,2816]{1,0:T(8,128)} %maximum_convert_fusion, f32[2816]{0:T(1024)S(1)} %get-tuple-element.9, f32[2816]{0:T(1024)S(1)} %get-tuple-element.10, f32[2816]{0:T(1024)S(1)} %get-tuple-element.8, ...), kind=kOutput, calls=%fused_computation.35 | convolution fusion | flops 11870928896 | bytes 85004288 | tf_op jit(solution)/shard_map/dot_general | solution.py:106
  515.7 53.8 %reduce-scatter.2.cloned.1.call-done = bf16[512,2048]{1,0:T(8,128)(2,1)} async-done(((bf16[1024,2048]{1,0:T(8,128)(2,1)}), bf16[512,2048]{1,0:T(8,128)(2,1)}) %reduce-scatter.2.cloned.1.call-update) | async-done | bytes 2097168 | tf_op jit(solution)/shard_map/reduce_scatter | solution.py:111
  569.4 3.7 fusion.17
  (42 shorter events, 0.9 us)
Async XLA Ops:
  6.5 21.5 %copy-start.1 = (bf16[1024,128]{1,0:T(8,128)(2,1)S(1)}, bf16[1024,128]{1,0:T(8,128)(2,1)}, u32[]{:S(2)}) copy-start(bf16[1024,128]{1,0:T(8,128)(2,1)} %param.14) | copy-start | bytes 786436
  6.5 81.9 %all-gather.7.cloned.1.call-start = ((), (), s32[]{:S(2)}) async-start(), calls=%async_computation.2 | async-start | bytes 6291456 | tf_op jit(solution)/shard_map/all_gather | solution.py:85
  7.8 19.8 %collective-permute-start.1 = (s32[128]{0:T(128)}, s32[128]{0:T(128)S(1)}, u32[]{:S(2)}, u32[]{:S(2)}) collective-permute-start(s32[128]{0:T(128)} %slice.83), channel_id=1, source_target_pairs={{0,2},{2,4},{4,6},{6,8},{8,10},{10,12},{12,14},{14,16},{16,18},{18... | collective-permute-start | bytes 1544 | tf_op jit(solution)/shard_map/ppermute | solution.py:13
  11.6 16.4 %collective-permute-start.2 = (bf16[128,128]{1,0:T(8,128)(2,1)}, bf16[128,128]{1,0:T(8,128)(2,1)S(1)}, u32[]{:S(2)}, u32[]{:S(2)}) collective-permute-start(bf16[128,128]{1,0:T(8,128)(2,1)} %slice.86), channel_id=1, source_target_pairs={{0,2},{2,4},{4,6},{6,8},{8,10},{10,12},{12,14},{14,16},{16,18},{18... | collective-permute-start | bytes 98312 | tf_op jit(solution)/shard_map/ppermute | solution.py:13
  16.9 11.7 %collective-permute-start = (bf16[128,128]{1,0:T(8,128)(2,1)S(1)}, bf16[128,128]{1,0:T(8,128)(2,1)S(1)}, u32[]{:S(2)}, u32[]{:S(2)}) collective-permute-start(bf16[128,128]{1,0:T(8,128)(2,1)S(1)} %slice.81), channel_id=1, source_target_pairs={{0,2},{2,4},{4,6},{6,8},{8,10},{10,12},{12,14},{14,16},{16,18},{18... | collective-permute-start | bytes 98312 | tf_op jit(solution)/shard_map/ppermute | solution.py:13
  18.8 134.1 %all-gather.9.cloned.1.call-start = ((), (), s32[]{:S(2)}) async-start(), calls=%async_computation.3 | async-start | bytes 6291456 | tf_op jit(solution)/shard_map/all_gather | solution.py:92
  30.3 5.1 copy-start.2
  39.0 55.1 %copy-start.5 = (f32[2048]{0:T(1024)S(1)}, f32[2048]{0:T(1024)}, u32[]{:S(2)}) copy-start(f32[2048]{0:T(1024)} %param.20) | copy-start | bytes 24580
  88.5 9.5 %copy-start.3 = (f32[3,2816]{1,0:T(4,128)S(1)}, f32[3,2816]{1,0:T(4,128)}, u32[]{:S(2)}) copy-start(f32[3,2816]{1,0:T(4,128)} %param.24) | copy-start | bytes 101380
  88.5 9.5 %copy-start.4 = (f32[3,2816]{1,0:T(4,128)S(1)}, f32[3,2816]{1,0:T(4,128)}, u32[]{:S(2)}) copy-start(f32[3,2816]{1,0:T(4,128)} %param.23) | copy-start | bytes 101380
  96.0 153.2 %all-gather.13.cloned.1.call-start = ((), (), s32[]{:S(2)}) async-start(), calls=%async_computation.5 | async-start | bytes 12255232 | tf_op jit(solution)/shard_map/all_gather | solution.py:98
  96.8 247.0 %all-gather.11.cloned.1.call-start = ((), (), s32[]{:S(2)}) async-start(), calls=%async_computation.4 | async-start | bytes 12255232 | tf_op jit(solution)/shard_map/all_gather | solution.py:97
  97.3 340.8 %all-gather.15.cloned.1.call-start = ((), (), s32[]{:S(2)}) async-start(), calls=%async_computation.7 | async-start | bytes 12255232 | tf_op jit(solution)/shard_map/all_gather | solution.py:108
  97.9 471.5 %reduce-scatter.2.cloned.1.call-start = ((), (), s32[]{:S(2)}) async-start(), calls=%async_computation.6 | async-start | bytes 6291456 | tf_op jit(solution)/shard_map/reduce_scatter | solution.py:111
  266.2 2.5 copy-start
  268.7 187.9 %collective-permute-start.4 = (bf16[2,2816]{1,0:T(2,128)(2,1)S(1)}, bf16[2,2816]{1,0:T(2,128)(2,1)S(1)}, u32[]{:S(2)}, u32[]{:S(2)}) collective-permute-start(bf16[2,2816]{1,0:T(2,128)(2,1)S(1)} %slice.111), channel_id=1, source_target_pairs={{0,2},{2,4},{4,6},{6,8},{8,10},{10,12},{12,14},{14,16},{16,18},{18... | collective-permute-start | bytes 33800 | tf_op jit(solution)/shard_map/ppermute | solution.py:13
  453.1 11.6 %slice-start = ((s8[5767168]{0:T(1024)(128)(4,1)}), s8[4194304]{0:T(1024)(128)(4,1)S(1)}, s32[]{:S(2)}) async-start(s8[5767168]{0:T(1024)(128)(4,1)} %bitcast.51), calls=%async_computation.8 | async-start | bytes 8388608
  454.1 10.7 %slice-start.1 = ((s8[5767168]{0:T(1024)(128)(4,1)}), s8[1572864]{0:T(1024)(128)(4,1)S(1)}, s32[]{:S(2)}) async-start(s8[5767168]{0:T(1024)(128)(4,1)} %bitcast.51), calls=%async_computation.9 | async-start | bytes 3145728
  454.1 10.6 %collective-permute-start.3 = (bf16[2,2816]{1,0:T(2,128)(2,1)S(1)}, bf16[2,2816]{1,0:T(2,128)(2,1)S(1)}, u32[]{:S(2)}, u32[]{:S(2)}) collective-permute-start(bf16[2,2816]{1,0:T(2,128)(2,1)S(1)} %slice.105), channel_id=1, source_target_pairs={{0,2},{2,4},{4,6},{6,8},{8,10},{10,12},{12,14},{14,16},{16,18},{18... | collective-permute-start | bytes 33800 | tf_op jit(solution)/shard_map/ppermute | solution.py:13
Sparse Core Ops, SparseCore 0:
  19.0 69.4 all-gather.6
  96.1 56.7 all-gather.8
  155.2 93.9 all-gather.12
  251.3 92.3 all-gather.10
  345.9 92.2 all-gather.14
  515.8 53.5 reduce-scatter.1
